TPU v7x, 32 devices: a whole 2x2x4 slice. The times are simulated.
32 devices in a mesh: dp: 4 (over y, x), kv: 4 (over z), tp: 2 (over core).
Axes of the slice: x: 2, y: 2, z: 4, core: 2. Of those that a mesh axis runs over, the one named last changes fastest.
Arguments:
- tokens: bfloat16 [256, 2048], P('dp', ('kv', 'tp')), parts along dimension 0, may hold values from -64 to 64, as said below
- lengths: int32 [32], P(('dp', 'kv', 'tp')), parts along dimension 0, may hold values from 1 to 8, 28 in all
- state: float32 [32, 16, 128, 128], P(('dp', 'kv', 'tp')), parts along dimension 0, may hold values from -1.8 to 1.8
- gain_first: float32 [2048], replicated, may hold values from 0.1 to 1.9
- first_gate: bfloat16 [2048, 5632], P(None, 'kv'), may hold values from -0.125 to 0.125
- first_up: bfloat16 [2048, 5632], P(None, 'kv'), may hold values from -0.125 to 0.125
- first_down: bfloat16 [5632, 2048], P('kv'), may hold values from -0.109375 to 0.109375
- gain_mix: float32 [2048], replicated, may hold values from 0.1 to 1.9
- query_weight: bfloat16 [2048, 2048], P(None, ('kv', 'tp')), may hold values from -0.125 to 0.125
- key_weight: bfloat16 [2048, 2048], P(None, ('kv', 'tp')), may hold values from -0.125 to 0.125
- value_weight: bfloat16 [2048, 2048], P(None, ('kv', 'tp')), may hold values from -0.125 to 0.125
- gating_weight: bfloat16 [2048, 2048], P(None, ('kv', 'tp')), may hold values from -0.125 to 0.125
- write_weight: bfloat16 [2048, 16], replicated, may hold values from -0.125 to 0.125
- forget_weight: bfloat16 [2048, 16], replicated, may hold values from -0.125 to 0.125
- forget_rate: float32 [16], replicated, may hold values from -4 to 1.5
- out_weight: bfloat16 [2048, 2048], P(None, ('kv', 'tp')), may hold values from -0.125 to 0.125
- gain_second: float32 [2048], replicated, may hold values from 0.1 to 1.9
- second_gate: bfloat16 [2048, 5632], P(None, 'kv'), may hold values from -0.125 to 0.125
- second_up: bfloat16 [2048, 5632], P(None, 'kv'), may hold values from -0.125 to 0.125
- second_down: bfloat16 [5632, 2048], P('kv'), may hold values from -0.109375 to 0.109375
Outputs:
- mixed_out: bfloat16 [256, 2048], P('dp', ('kv', 'tp')), parts along dimension 0
- new_state: float32 [32, 16, 128, 128], P(('dp', 'kv', 'tp')), parts along dimension 0
There are 4 independent parts, one for each index of `dp`. A program takes and returns all parts, laid end to end along the dimension named above; an argument that names none is the same for every part. Nothing has to cross between parts.
Inputs may be any that keep to these rules, and one draw needn't show every extreme that they name: Activations of the new tokens. `lengths`: the live new tokens of each sequence; within each independent group of 8 sequences (one part along dp) they sum to seven halves of 8, rounded down, and some sequence of each group has all 8 live.
All inputs are finite; a program needn't handle non-finite values.
Results may differ from a plain program's by a relative error of at most 0.0058.
Values may be sent and summed in bfloat16 or wider, within the bound.
A program may use at most 128 MiB of HBM per device.

v0:
```python
import math

import jax
import jax.numpy as jnp
from jax import lax
from jax.sharding import PartitionSpec as P

HEADS = 16
HEAD = 128
BLK = 8


EPSILON = 1e-06


def fold_step(gain, gate_cols, up_cols, portion):
    values = portion.astype(jnp.float32)
    scaled = (values * gain).astype(jnp.bfloat16)
    gate_acc = jnp.dot(scaled, gate_cols, preferred_element_type=jnp.float32)
    up_acc = jnp.dot(scaled, up_cols, preferred_element_type=jnp.float32)
    squares = jnp.sum(values * values, axis=1)
    return (gate_acc, up_acc, squares)


def finish_units(gate_acc, up_acc, squares, channels, down_rows):
    row_scale = lax.rsqrt(squares / channels + EPSILON)[:, None]
    hidden = (jax.nn.silu(gate_acc * row_scale) * (up_acc * row_scale)).astype(jnp.bfloat16)
    return jnp.dot(hidden, down_rows, preferred_element_type=jnp.float32)


def feed_forward(hidden_in, gain, w_gate, w_up, w_down):
    channels = gain.shape[0]
    paired = lax.all_to_all(hidden_in, "tp", split_axis=0, concat_axis=1, tiled=True)
    gate_acc, up_acc, squares = fold_step(
        gain, w_gate, w_up, lax.all_gather(paired, "kv", axis=1, tiled=True)
    )
    ffn_term = finish_units(gate_acc, up_acc, squares, channels, w_down)
    partial_value = lax.psum_scatter(ffn_term, "kv", scatter_dimension=1, tiled=True)
    summed = lax.all_to_all(partial_value, "tp", split_axis=1, concat_axis=0, tiled=True)
    return (hidden_in.astype(jnp.float32) + 0.5 * summed).astype(jnp.bfloat16)


def delta_block(query, key_in, value, gating, write_pre, forget_pre, rates, live, state):
    seq_count, block_len, head_count, head_size = query.shape
    precise = lax.Precision.HIGHEST
    query_unit = (
        query
        * lax.rsqrt(jnp.sum(query * query, axis=-1, keepdims=True) + EPSILON)
        / math.sqrt(head_size)
    )
    key_unit = key_in * lax.rsqrt(jnp.sum(key_in * key_in, axis=-1, keepdims=True) + EPSILON)
    live_rows = live[:, :, None]
    write_gate = jax.nn.sigmoid(write_pre) * live_rows
    forget = -jnp.exp(rates)[None, None, :] * jax.nn.softplus(forget_pre) * live_rows
    cumulative = jnp.cumsum(forget, axis=1)
    cum_heads = jnp.transpose(cumulative, (0, 2, 1))
    positions = jnp.arange(block_len)
    causal = positions[:, None] >= positions[None, :]
    strict = positions[:, None] > positions[None, :]
    differ = jnp.minimum(cum_heads[:, :, :, None] - cum_heads[:, :, None, :], 0.0)
    decay_mat = jnp.where(causal, jnp.exp(differ), 0.0)
    key_dots = jnp.einsum("sthd,suhd->shtu", key_unit, key_unit, precision=precise)
    write_heads = jnp.transpose(write_gate, (0, 2, 1))
    strict_part = jnp.where(strict, write_heads[:, :, :, None] * decay_mat * key_dots, 0.0)
    identity = jnp.eye(block_len, dtype=jnp.float32)
    squared = jnp.einsum("shtu,shuv->shtv", strict_part, strict_part, precision=precise)
    fourth = jnp.einsum("shtu,shuv->shtv", squared, squared, precision=precise)
    inverse = jnp.einsum(
        "shtu,shuv->shtv", identity - strict_part, identity + squared, precision=precise
    )
    inverse = jnp.einsum("shtu,shuv->shtv", inverse, identity + fourth, precision=precise)
    growth = jnp.exp(cumulative)
    target = jnp.einsum(
        "shtu,suhv->sthv", inverse, write_gate[..., None] * value, precision=precise
    )
    key_mix = jnp.einsum(
        "shtu,suhk->sthk", inverse, (write_gate * growth)[..., None] * key_unit, precision=precise
    )
    update = target - jnp.einsum("sthk,shkv->sthv", key_mix, state, precision=precise)
    scores = jnp.einsum("sthd,suhd->shtu", query_unit, key_unit, precision=precise) * decay_mat
    attend = jnp.einsum("sthk,shkv->sthv", query_unit * growth[..., None], state, precision=precise)
    attend = attend + jnp.einsum("shtu,suhv->sthv", scores, update, precision=precise)
    final_cum = cumulative[:, -1:, :]
    fading = jnp.exp(final_cum - cumulative)
    new_state = jnp.exp(final_cum[:, 0, :])[:, :, None, None] * state
    new_state = new_state + jnp.einsum(
        "sthk,sthv->shkv", key_unit * fading[..., None], update, precision=precise
    )
    normed = attend * lax.rsqrt(jnp.mean(attend * attend, axis=-1, keepdims=True) + EPSILON)
    normed = normed * jax.nn.silu(gating) * live[:, :, None, None]
    mixed_heads = normed.reshape(seq_count * block_len, head_count * head_size).astype(jnp.bfloat16)
    return (mixed_heads, new_state)


def per_device(
    tokens,
    lengths,
    state,
    gain_first,
    first_gate,
    first_up,
    first_down,
    gain_mix,
    query_weight,
    key_weight,
    value_weight,
    gating_weight,
    write_weight,
    forget_weight,
    forget_rate,
    out_weight,
    gain_second,
    second_gate,
    second_up,
    second_down,
):
    after_first = feed_forward(tokens, gain_first, first_gate, first_up, first_down)
    seq_count = lengths.shape[0]
    own_count = seq_count * BLK
    whole_rows = lax.all_gather(after_first, ("kv", "tp"), axis=1, tiled=True)
    scaled_all = (whole_rows.astype(jnp.float32) * gain_mix).astype(jnp.bfloat16)
    stacked = jnp.stack(
        [
            jnp.dot(scaled_all, matrix, preferred_element_type=jnp.float32)
            for matrix in (query_weight, key_weight, value_weight, gating_weight)
        ]
    )
    owned = lax.all_to_all(
        stacked.astype(jnp.bfloat16), ("kv", "tp"), split_axis=1, concat_axis=2, tiled=True
    ).astype(stacked.dtype)
    row_start = lax.axis_index(("kv", "tp")) * own_count
    own_values = lax.dynamic_slice_in_dim(whole_rows, row_start, own_count, 0).astype(jnp.float32)
    own_scaled = lax.dynamic_slice_in_dim(scaled_all, row_start, own_count, 0)
    mix_scale = lax.rsqrt(jnp.mean(own_values * own_values, axis=1, keepdims=True) + EPSILON)
    query = (owned[0] * mix_scale).reshape(seq_count, BLK, HEADS, HEAD)
    key_in = (owned[1] * mix_scale).reshape(seq_count, BLK, HEADS, HEAD)
    value = (owned[2] * mix_scale).reshape(seq_count, BLK, HEADS, HEAD)
    gating = (owned[3] * mix_scale).reshape(seq_count, BLK, HEADS, HEAD)
    write_pre = (
        jnp.dot(own_scaled, write_weight, preferred_element_type=jnp.float32) * mix_scale
    ).reshape(seq_count, BLK, HEADS)
    forget_pre = (
        jnp.dot(own_scaled, forget_weight, preferred_element_type=jnp.float32) * mix_scale
    ).reshape(seq_count, BLK, HEADS)
    positions = jnp.arange(BLK, dtype=jnp.int32)
    live = (positions[None, :] < lengths[:, None]).astype(jnp.float32)
    mixed_heads, new_state = delta_block(
        query, key_in, value, gating, write_pre, forget_pre, forget_rate, live, state
    )
    half_cols = mixed_heads.shape[1] // 2
    portion = lax.all_gather(mixed_heads, ("kv", "tp"), axis=0, tiled=True)
    first_half = jnp.dot(
        portion[:, :half_cols], out_weight[:half_cols], preferred_element_type=jnp.float32
    ).astype(jnp.bfloat16)
    second_half = jnp.dot(
        portion[:, half_cols:], out_weight[half_cols:], preferred_element_type=jnp.float32
    ).astype(jnp.bfloat16)
    first_half, second_half = lax.optimization_barrier((first_half, second_half))
    mixed_sum = first_half.astype(jnp.float32) + second_half.astype(jnp.float32)
    after_mix = (after_first.astype(jnp.float32) + mixed_sum).astype(jnp.bfloat16)
    mixed_out = feed_forward(after_mix, gain_second, second_gate, second_up, second_down)
    return (mixed_out, new_state)


def solution(mesh):
    in_specs = (
        P("dp", ("kv", "tp")),
        P(("dp", "kv", "tp")),
        P(("dp", "kv", "tp"), None, None, None),
        P(),
        P(None, "kv"),
        P(None, "kv"),
        P("kv", None),
        P(),
        P(None, ("kv", "tp")),
        P(None, ("kv", "tp")),
        P(None, ("kv", "tp")),
        P(None, ("kv", "tp")),
        P(),
        P(),
        P(),
        P(None, ("kv", "tp")),
        P(),
        P(None, "kv"),
        P(None, "kv"),
        P("kv", None),
    )
    out_specs = (P("dp", ("kv", "tp")), P(("dp", "kv", "tp"), None, None, None))
    return jax.shard_map(
        per_device, mesh=mesh, in_specs=in_specs, out_specs=out_specs, check_vma=False
    )
```

profile of v0, /device:TPU:0, one launch (start us, length us, event | category | flops | bytes accessed | tf_op | source)
XLA Modules:
  0.0 174.8 jit_solution(16179178874863830319)
XLA Ops:
  7.2 4.8 %all_to_all.73 = bf16[2,32,256]{2,1,0:T(8,128)(2,1)S(1)} all-to-all(bf16[2,32,256]{2,1,0:T(8,128)(2,1)} %bitcast.150), channel_id=1, replica_groups=mesh['dp'=4,'kv'=4,'tp'=2] {'tp'}, dimensions={0} | all-to-all | bytes 65536 | tf_op jit(solution)/shard_map/all_to_all | solution.py:33
  12.0 15.1 %all_gather.12 = bf16[32,2048]{1,0:T(8,128)(2,1)S(1)} all-gather(bf16[32,512]{1,0:T(8,128)(2,1)S(1)} %bitcast.146), channel_id=1, replica_groups=mesh['dp'=4,'kv'=4,'tp'=2] {'kv'}, dimensions={1}, use_global_device_ids=true | all-gather | bytes 163840 | tf_op jit(solution)/shard_map/all_gather | solution.py:35
  27.2 3.7 %convolution_multiply_fusion.3 = f32[32,1408]{1,0:T(8,128)S(1)} fusion(bf16[2048,1408]{1,0:T(8,128)(2,1)} %param.24, bf16[32,2048]{1,0:T(8,128)(2,1)S(1)} %all_gather.12, f32[2048]{0:T(1024)} %param.23, f32[32]{0:T(128)S(1)} %add_rsqrt_fusion.5), kind=kOutput, calls=%fused_computation.5 | convolution fusion | flops 184791040 | bytes 6086784 | tf_op jit(solution)/shard_map/dot_general | solution.py:19
  31.0 7.1 %fusion.21 = f32[32,2048]{1,0:T(8,128)} fusion(bf16[1408,2048]{1,0:T(8,128)(2,1)} %param.26, bf16[2048,1408]{1,0:T(8,128)(2,1)} %param.25, f32[32,1408]{1,0:T(8,128)S(1)} %convolution_multiply_fusion.3, bf16[32,2048]{1,0:T(8,128)(2,1)S(1)} %all_gather.12, f32[2048]{0:T(1024)S(1)} %copy-done.4, f32[32]{0:T(128)S(1)} %add_rsqrt_fusion.5), kind=kOutput, calls=%fused_computation.41 | convolution fusion | flops 369610752 | bytes 12116096 | tf_op jit(solution)/shard_map/dot_general | solution.py:28
  38.9 20.5 %reduce-scatter.3.cloned.1.call-done = f32[32,512]{1,0:T(8,128)} async-done(((f32[32,2048]{1,0:T(8,128)}), f32[32,512]{1,0:T(8,128)}) %reduce-scatter.3.cloned.1.call-update) | async-done | bytes 65552 | tf_op jit(solution)/shard_map/reduce_scatter | solution.py:38
  59.4 0.8 copy.159
  60.2 3.8 %all_to_all.74 = f32[32,2,256]{2,0,1:T(8,128)S(1)} all-to-all(f32[32,2,256]{2,0,1:T(8,128)S(1)} %bitcast.144), channel_id=1, replica_groups=mesh['dp'=4,'kv'=4,'tp'=2] {'tp'}, dimensions={1} | all-to-all | bytes 131072 | tf_op jit(solution)/shard_map/all_to_all | solution.py:39
  64.0 14.3 %all_gather.13 = bf16[64,2048]{1,0:T(8,128)(2,1)S(1)} all-gather(bf16[64,256]{1,0:T(8,128)(2,1)S(1)} %fusion.51), channel_id=1, replica_groups=mesh['dp'=4,'kv'=4,'tp'=2] {'kv','tp'}, dimensions={1}, use_global_device_ids=true | all-gather | bytes 294912 | tf_op jit(solution)/shard_map/all_gather | solution.py:120
  78.6 0.3 fusion.12
  78.9 0.3 fusion.11
  79.2 1.5 fusion.10
  80.7 1.5 fusion.9
  82.3 0.8 copy.99
  83.0 3.4 %all-to-all-start.2 = ((bf16[4,64,256]{2,0,1:T(4,128)(2,1)}), bf16[4,64,256]{2,0,1:T(4,128)(2,1)S(1)}, u32[]{:S(2)}, u32[]{:S(2)}) async-start(bf16[4,64,256]{2,0,1:T(4,128)(2,1)} %copy.99), calls=%async_computation.3 | async-start | bytes 262144 | tf_op jit(solution)/shard_map/all_to_all | solution.py:128
  86.7 0.9 fusion.80
  87.8 5.3 %all-to-all-done.2 = bf16[4,64,256]{2,0,1:T(4,128)(2,1)S(1)} async-done(((bf16[4,64,256]{2,0,1:T(4,128)(2,1)}), bf16[4,64,256]{2,0,1:T(4,128)(2,1)S(1)}, u32[]{:S(2)}, u32[]{:S(2)}) %all-to-all-start.2) | async-done | bytes 131104 | tf_op jit(solution)/shard_map/all_to_all | solution.py:128
  94.8 0.3 convolution_multiply_fusion.4
  96.0 1.0 convolution_bitcast_fusion.3
  96.9 1.0 fusion.7
  97.9 0.3 multiply_reduce_fusion
  98.5 14.2 %all_gather.14 = bf16[64,2048]{1,0:T(8,128)(2,1)S(1)} all-gather(bf16[8,2048]{1,0:T(8,128)(2,1)S(1)} %fusion.70), channel_id=1, replica_groups=mesh['dp'=4,'kv'=4,'tp'=2] {'kv','tp'}, dimensions={0}, use_global_device_ids=true | all-gather | bytes 294912 | tf_op jit(solution)/shard_map/all_gather | solution.py:151
  112.8 1.2 convolution_convert_fusion
  114.0 1.2 convolution_convert_fusion.1
  115.3 3.7 %all_to_all.75 = bf16[2,32,256]{2,1,0:T(8,128)(2,1)S(1)} all-to-all(bf16[2,32,256]{2,1,0:T(8,128)(2,1)S(1)} %bitcast.143), channel_id=1, replica_groups=mesh['dp'=4,'kv'=4,'tp'=2] {'tp'}, dimensions={0} | all-to-all | bytes 65536 | tf_op jit(solution)/shard_map/all_to_all | solution.py:33
  119.0 13.6 %all_gather.15 = bf16[32,2048]{1,0:T(8,128)(2,1)S(1)} all-gather(bf16[32,512]{1,0:T(8,128)(2,1)S(1)} %bitcast.147), channel_id=1, replica_groups=mesh['dp'=4,'kv'=4,'tp'=2] {'kv'}, dimensions={1}, use_global_device_ids=true | all-gather | bytes 163840 | tf_op jit(solution)/shard_map/all_gather | solution.py:35
  132.7 3.6 %convolution_multiply_fusion.1 = f32[32,1408]{1,0:T(8,128)S(1)} fusion(bf16[2048,1408]{1,0:T(8,128)(2,1)} %param.37, bf16[32,2048]{1,0:T(8,128)(2,1)S(1)} %all_gather.15, f32[2048]{0:T(1024)S(1)} %copy-done.5, f32[32]{0:T(128)S(1)} %add_rsqrt_fusion.3), kind=kOutput, calls=%fused_computation.2 | convolution fusion | flops 184791040 | bytes 6086784 | tf_op jit(solution)/shard_map/dot_general | solution.py:19
  136.4 7.0 %fusion.20 = f32[32,2048]{1,0:T(8,128)} fusion(bf16[1408,2048]{1,0:T(8,128)(2,1)} %param.39, bf16[2048,1408]{1,0:T(8,128)(2,1)} %param.38, f32[32,1408]{1,0:T(8,128)S(1)} %convolution_multiply_fusion.1, bf16[32,2048]{1,0:T(8,128)(2,1)S(1)} %all_gather.15, f32[2048]{0:T(1024)S(1)} %copy-done.5, f32[32]{0:T(128)S(1)} %add_rsqrt_fusion.3), kind=kOutput, calls=%fused_computation.40 | convolution fusion | flops 369610752 | bytes 12116096 | tf_op jit(solution)/shard_map/dot_general | solution.py:28
  143.5 2.8 %fusion.4 = f32[1,16,128,128]{3,2,1,0:T(8,128)} fusion(f32[8,16,128]{2,0,1:T(8,128)S(1)} %fusion.7, f32[1,16,128,128]{3,2,1,0:T(8,128)S(1)} %copy-done.1, f32[16]{0:T(128)S(1)} %fusion.86, f32[8,16,128]{2,1,0:T(8,128)S(1)} %get-tuple-element.20), kind=kOutput, calls=%fused_computation.9 | convolution fusion | flops 25690112 | bytes 2228288 | tf_op jit(solution)/shard_map/sthk,sthv->shkv/dot_general | solution.py:86
  146.3 16.4 %reduce-scatter.5.cloned.1.call-done = f32[32,512]{1,0:T(8,128)} async-done(((f32[32,2048]{1,0:T(8,128)}), f32[32,512]{1,0:T(8,128)}) %reduce-scatter.5.cloned.1.call-update) | async-done | bytes 65552 | tf_op jit(solution)/shard_map/reduce_scatter | solution.py:38
  162.7 0.8 copy.158
  163.6 3.8 %all_to_all.76 = f32[32,2,256]{2,0,1:T(8,128)S(1)} all-to-all(f32[32,2,256]{2,0,1:T(8,128)S(1)} %bitcast.145), channel_id=1, replica_groups=mesh['dp'=4,'kv'=4,'tp'=2] {'tp'}, dimensions={1} | all-to-all | bytes 131072 | tf_op jit(solution)/shard_map/all_to_all | solution.py:39
  167.4 0.6 fusion.50
  (71 shorter events, 3.8 us)
Async XLA Ops:
  7.2 71.4 %copy-start = (bf16[2048,256]{1,0:T(8,128)(2,1)S(1)}, bf16[2048,256]{1,0:T(8,128)(2,1)}, u32[]{:S(2)}) copy-start(bf16[2048,256]{1,0:T(8,128)(2,1)} %param.31) | copy-start | bytes 3145732
  7.2 23.7 %copy-start.4 = (f32[2048]{0:T(1024)S(1)}, f32[2048]{0:T(1024)}, u32[]{:S(2)}) copy-start(f32[2048]{0:T(1024)} %param.23) | copy-start | bytes 24580
  7.2 52.2 %reduce-scatter.3.cloned.1.call-start = ((), (), s32[]{:S(2)}) async-start(), calls=%async_computation.7 | async-start | bytes 327680 | tf_op jit(solution)/shard_map/reduce_scatter | solution.py:38
  30.9 7.9 %copy-start.8 = (f32[16]{0:T(128)S(1)}, f32[16]{0:T(128)}, u32[]{:S(2)}) copy-start(f32[16]{0:T(128)} %param.34) | copy-start | bytes 196
  30.9 33.1 %copy-start.3 = (bf16[64,256]{1,0:T(8,128)(2,1)S(1)}, bf16[64,256]{1,0:T(8,128)(2,1)}, u32[]{:S(2)}) copy-start(bf16[64,256]{1,0:T(8,128)(2,1)} %param.20) | copy-start | bytes 98308
  30.9 47.6 %copy-start.6 = (f32[2048]{0:T(1024)S(1)}, f32[2048]{0:T(1024)}, u32[]{:S(2)}) copy-start(f32[2048]{0:T(1024)} %param.27) | copy-start | bytes 24580
  30.9 47.9 %copy-start.2 = (bf16[2048,256]{1,0:T(8,128)(2,1)S(1)}, bf16[2048,256]{1,0:T(8,128)(2,1)}, u32[]{:S(2)}) copy-start(bf16[2048,256]{1,0:T(8,128)(2,1)} %param.30) | copy-start | bytes 3145732
  38.1 48.4 %copy-start.7 = (bf16[2048,16]{0,1:T(8,128)(2,1)S(1)}, bf16[2048,16]{0,1:T(8,128)(2,1)}, u32[]{:S(2)}) copy-start(bf16[2048,16]{0,1:T(8,128)(2,1)} %param.33) | copy-start | bytes 196612
  64.0 31.9 %copy-start.1 = (f32[1,16,128,128]{3,2,1,0:T(8,128)S(1)}, f32[1,16,128,128]{3,2,1,0:T(8,128)}, u32[]{:S(2)}) copy-start(f32[1,16,128,128]{3,2,1,0:T(8,128)} %param.22) | copy-start | bytes 3145732
  80.7 52.0 %copy-start.5 = (f32[2048]{0:T(1024)S(1)}, f32[2048]{0:T(1024)}, u32[]{:S(2)}) copy-start(f32[2048]{0:T(1024)} %param.36) | copy-start | bytes 24580
  83.0 10.1 %all-to-all-start.2 = ((bf16[4,64,256]{2,0,1:T(4,128)(2,1)}), bf16[4,64,256]{2,0,1:T(4,128)(2,1)S(1)}, u32[]{:S(2)}, u32[]{:S(2)}) async-start(bf16[4,64,256]{2,0,1:T(4,128)(2,1)} %copy.99), calls=%async_computation.3 | async-start | bytes 262144 | tf_op jit(solution)/shard_map/all_to_all | solution.py:128
  86.4 76.3 %reduce-scatter.5.cloned.1.call-start = ((), (), s32[]{:S(2)}) async-start(), calls=%async_computation.8 | async-start | bytes 327680 | tf_op jit(solution)/shard_map/reduce_scatter | solution.py:38
Sparse Core Ops, SparseCore 0:
  38.2 21.0 reduce-scatter.2
  143.6 19.1 reduce-scatter.4
where the time goes:
time: 176 us; the launch traced here: 175 us
  blocking collectives  73.2 us (42%)
  waiting for transfers between devices  42.3 us (24%)
  matrix products  35.8 us (20%)
  between operations  15.2 us (9%)
  starting transfers between devices  3.45 us (2%)
  local copies, waits for them, and re-layouts  3.13 us (2%)
  other arithmetic  1.76 us (1%)
    reduce_scatter x2, waiting for transfers between devices, feed_forward(): lax.psum_scatter(ffn_term, 'kv', scatter_dimension=1, tiled=True)  36.9 us
    all_gather x2, blocking collectives, feed_forward(): lax.all_gather(paired, 'kv', axis=1, tiled=True)  28.6 us
    all_gather x1, blocking collectives, per_device(): whole_rows = lax.all_gather(after_first, ('kv', 'tp'), axis=1, tiled=True)  14.3 us
    all_gather x1, blocking collectives, per_device(): portion = lax.all_gather(mixed_heads, ('kv', 'tp'), axis=0, tiled=True)  14.2 us
    dot_general x2, matrix products, finish_units(): return jnp.dot(hidden, down_rows, preferred_element_type=jnp.float32)  14.2 us
    all_to_all x2, blocking collectives, feed_forward(): lax.all_to_all(hidden_in, 'tp', split_axis=0, concat_axis=1, tiled=True)  8.52 us
    all_to_all x2, blocking collectives, feed_forward(): lax.all_to_all(partial_value, 'tp', split_axis=1, concat_axis=0, tiled=True)  7.56 us
    dot_general x2, matrix products, fold_step(): gate_acc = jnp.dot(scaled, gate_cols, preferred_element_type=jnp.float32)  7.31 us
  transfers between devices with their start and end apart: 3, of which 3 were waited for; matrix products, arithmetic and copies ran while one was open for 2% of the time, Pallas kernels for 0%

commit v1 on v0

--- a/solution.py
+++ b/solution.py
@@ -1,8 +1,11 @@
+import functools
 import math
 
 import jax
 import jax.numpy as jnp
 from jax import lax
+from jax.experimental import pallas as pl
+from jax.experimental.pallas import tpu as pltpu
 from jax.sharding import PartitionSpec as P
 
 HEADS = 16
@@ -162,6 +165,476 @@
     return (mixed_out, new_state)
 
 
+F32 = jnp.float32
+BF16 = jnp.bfloat16
+HIGH = lax.Precision.HIGHEST
+MESH = pl.DeviceIdType.MESH
+VMEM_LIMIT = 60 * 1024 * 1024
+
+
+def fused_kernel(
+    kv_size,
+    channels,
+    tokens_ref,
+    lengths_ref,
+    gains1_ref,
+    gains_mix_ref,
+    gains2_ref,
+    rates_ref,
+    state_hbm,
+    gate1_hbm,
+    up1_hbm,
+    down1_hbm,
+    query_hbm,
+    key_hbm,
+    value_hbm,
+    gating_hbm,
+    write_hbm,
+    forget_hbm,
+    out_hbm,
+    gate2_hbm,
+    up2_hbm,
+    down2_hbm,
+    mixed_out_ref,
+    new_state_hbm,
+    gate1,
+    up1,
+    down1,
+    gate2,
+    up2,
+    down2,
+    proj,
+    out_w,
+    write_w,
+    forget_w,
+    state,
+    state_out,
+    scaled,
+    wide,
+    narrow,
+    gathers,
+    heads_all,
+    pair_send,
+    pair_recv,
+    red_send,
+    red_recv,
+    part_send,
+    part_recv,
+    load_sems,
+    gather_send_sems,
+    gather_recv_sems,
+    pair_send_sems,
+    pair_recv_sems,
+    red_send_sems,
+    red_recv_sems,
+    part_send_sems,
+    part_recv_sems,
+    store_sem,
+):
+    kv = lax.axis_index("kv")
+    tp = lax.axis_index("tp")
+    devices = 2 * kv_size
+    me = kv * 2 + tp
+    rows, cols = tokens_ref.shape
+    take = gate1.shape[1]
+    hidden_local = gate1_hbm.shape[1]
+    lead = hidden_local - take
+    overlap = 2 * take - hidden_local
+    first_col = pl.multiple_of(tp * lead, 128)
+
+    def load(index, src, dst):
+        return pltpu.make_async_copy(src, dst, load_sems.at[index])
+
+    cut = pl.ds(first_col, take)
+    loads = {
+        "gate1": load(0, gate1_hbm.at[:, cut], gate1),
+        "up1": load(1, up1_hbm.at[:, cut], up1),
+        "down1": load(2, down1_hbm.at[cut, :], down1),
+        "query": load(3, query_hbm, proj.at[0]),
+        "key": load(4, key_hbm, proj.at[1]),
+        "value": load(5, value_hbm, proj.at[2]),
+        "gating": load(6, gating_hbm, proj.at[3]),
+        "write": load(7, write_hbm, write_w),
+        "forget": load(8, forget_hbm, forget_w),
+        "state": load(9, state_hbm.at[0], state),
+        "out": load(10, out_hbm, out_w),
+        "gate2": load(11, gate2_hbm.at[:, cut], gate2),
+        "up2": load(12, up2_hbm.at[:, cut], up2),
+        "down2": load(13, down2_hbm.at[cut, :], down2),
+    }
+    for name in ("gate1", "up1", "down1"):
+        loads[name].start()
+
+    def remote(src, dst, send_sem, recv_sem, to_kv, to_tp):
+        return pltpu.make_async_remote_copy(
+            src_ref=src,
+            dst_ref=dst,
+            send_sem=send_sem,
+            recv_sem=recv_sem,
+            device_id={"kv": to_kv, "tp": to_tp},
+            device_id_type=MESH,
+        )
+
+    barrier = pltpu.get_barrier_semaphore()
+    for off in range(1, devices):
+        peer = lax.rem(me + off, devices)
+        pl.semaphore_signal(
+            barrier,
+            inc=1,
+            device_id={"kv": peer // 2, "tp": lax.rem(peer, 2)},
+            device_id_type=MESH,
+        )
+    pl.semaphore_wait(barrier, devices - 1)
+
+    def gather_start(phase, buf):
+        copies = []
+        for off in range(kv_size - 1, 0, -1):
+            copies.append(
+                remote(
+                    buf.at[me],
+                    buf.at[me],
+                    gather_send_sems.at[phase, off],
+                    gather_recv_sems.at[phase, off],
+                    lax.rem(kv + off, kv_size),
+                    tp,
+                )
+            )
+        copies.append(
+            remote(
+                buf.at[me],
+                buf.at[me],
+                gather_send_sems.at[phase, 0],
+                gather_recv_sems.at[phase, 0],
+                kv,
+                1 - tp,
+            )
+        )
+        for copy in copies:
+            copy.start()
+        return copies
+
+    def gather_finish(phase, buf, copies):
+        forwards = []
+        for off in range(1, kv_size):
+            copies[kv_size - 1 - off].wait_recv()
+            slot = lax.rem(kv + kv_size - off, kv_size) * 2 + tp
+            forward = remote(
+                buf.at[slot],
+                buf.at[slot],
+                gather_send_sems.at[phase, kv_size - 1 + off],
+                gather_recv_sems.at[phase, kv_size - 1 + off],
+                kv,
+                1 - tp,
+            )
+            forward.start()
+            forwards.append(forward)
+        copies[-1].wait_recv()
+        for forward in forwards:
+            forward.wait_recv()
+        for copy in copies + forwards:
+            copy.wait_send()
+
+    def scale_rows(buf, gain_ref):
+        squares = jnp.zeros((rows, 1), F32)
+        for j in range(devices):
+            values = buf[j].astype(F32)
+            squares = squares + jnp.sum(values * values, axis=1, keepdims=True)
+            gain = gain_ref[:, j * cols : (j + 1) * cols]
+            scaled[:, j * cols : (j + 1) * cols] = (values * gain).astype(BF16)
+        return lax.rsqrt(squares / channels + EPSILON)
+
+    def half_step(phase, buf, gain_ref, names, gate_w, up_w, down_w):
+        row_scale = scale_rows(buf, gain_ref)
+        loads[names[0]].wait()
+        gate = jnp.dot(scaled[...], gate_w[...], preferred_element_type=F32) * row_scale
+        loads[names[1]].wait()
+        up = jnp.dot(scaled[...], up_w[...], preferred_element_type=F32) * row_scale
+        column = lax.broadcasted_iota(jnp.int32, (rows, take), 1)
+        hidden = jnp.where(column >= tp * overlap, jax.nn.silu(gate) * up, 0.0).astype(BF16)
+        loads[names[2]].wait()
+
+        def columns_of(chip, core):
+            at = pl.multiple_of((chip * 2 + core) * cols, cols)
+            return jnp.dot(hidden, down_w[:, pl.ds(at, cols)], preferred_element_type=F32)
+
+        order = list(range(kv_size - 1, -1, -1))
+        pair_copies = []
+        for off in order:
+            pair_send[phase, off] = columns_of(lax.rem(kv + off, kv_size), 1 - tp)
+            copy = remote(
+                pair_send.at[phase, off],
+                pair_recv.at[phase, off],
+                pair_send_sems.at[phase, off],
+                pair_recv_sems.at[phase, off],
+                kv,
+                1 - tp,
+            )
+            copy.start()
+            pair_copies.append(copy)
+        red_copies = []
+        total = None
+        for position, off in enumerate(order):
+            term = columns_of(lax.rem(kv + off, kv_size), tp)
+            pair_copies[position].wait_recv()
+            term = term + pair_recv[phase, off]
+            if off == 0:
+                total = term
+                continue
+            red_send[phase, off] = term.astype(BF16)
+            copy = remote(
+                red_send.at[phase, off],
+                red_recv.at[phase, off],
+                red_send_sems.at[phase, off],
+                red_recv_sems.at[phase, off],
+                lax.rem(kv + off, kv_size),
+                tp,
+            )
+            copy.start()
+            red_copies.append(copy)
+        for copy in red_copies[::-1]:
+            copy.wait_recv()
+        for off in range(1, kv_size):
+            total = total + red_recv[phase, off].astype(F32)
+        for copy in pair_copies + red_copies:
+            copy.wait_send()
+        return total
+
+    gathers[0, me] = tokens_ref[...]
+    copies = gather_start(0, gathers.at[0])
+    for name in ("query", "key", "value", "gating", "write", "forget", "state", "out"):
+        loads[name].start()
+    gather_finish(0, gathers.at[0], copies)
+    for name in ("gate2", "up2", "down2"):
+        loads[name].start()
+    total = half_step(0, gathers.at[0], gains1_ref, ("gate1", "up1", "down1"), gate1, up1, down1)
+    after_first = (tokens_ref[...].astype(F32) + 0.5 * total).astype(BF16)
+    gathers[1, me] = after_first
+    copies = gather_start(1, gathers.at[1])
+    gather_finish(1, gathers.at[1], copies)
+
+    mix_scale = scale_rows(gathers.at[1], gains_mix_ref)
+    for index, name in enumerate(("query", "key", "value", "gating")):
+        loads[name].wait()
+        product = jnp.dot(scaled[...], proj[index], preferred_element_type=F32) * mix_scale
+        part_send[:, :, index * cols : (index + 1) * cols] = product.reshape(
+            devices, BLK, cols
+        ).astype(BF16)
+    part_copies = []
+    for off in range(1, devices):
+        peer = lax.rem(me + off, devices)
+        copy = remote(
+            part_send.at[peer],
+            part_recv.at[me],
+            part_send_sems.at[off],
+            part_recv_sems.at[off],
+            peer // 2,
+            lax.rem(peer, 2),
+        )
+        copy.start()
+        part_copies.append(copy)
+    part_recv[me] = part_send[me]
+    loads["write"].wait()
+    loads["forget"].wait()
+    wide[:, 0:HEADS] = jnp.dot(scaled[...], write_w[...], preferred_element_type=F32) * mix_scale
+    narrow[:, 0:HEADS] = jnp.dot(scaled[...], forget_w[...], preferred_element_type=F32) * mix_scale
+    own = pl.ds(pl.multiple_of(me * BLK, BLK), BLK)
+    write_pre = wide[own, 0:HEADS]
+    forget_pre = narrow[own, 0:HEADS]
+
+    size = HEADS * BLK
+    row = lax.broadcasted_iota(jnp.int32, (size, size), 0)
+    col = lax.broadcasted_iota(jnp.int32, (size, size), 1)
+    same = (row // BLK) == (col // BLK)
+    causal = same & (row >= col)
+    strict = same & (row > col)
+    diagonal = row == col
+    identity = jnp.where(diagonal, 1.0, 0.0)
+    head_row = lax.broadcasted_iota(jnp.int32, (size, HEADS), 0) // BLK
+    head_col = lax.broadcasted_iota(jnp.int32, (size, HEADS), 1)
+    pick = head_row == head_col
+
+    def as_column(block):
+        return jnp.sum(jnp.where(pick, block, 0.0), axis=1, keepdims=True)
+
+    def to_row(column):
+        return jnp.sum(jnp.where(diagonal, column, 0.0), axis=0, keepdims=True)
+
+    token_at = lax.rem(lax.broadcasted_iota(jnp.int32, (size, 1), 0), BLK)
+    live = jnp.where(token_at < lengths_ref[0], 1.0, 0.0)
+    write_col = as_column(jnp.concatenate([write_pre] * HEADS, axis=0))
+    forget_col = as_column(jnp.concatenate([forget_pre] * HEADS, axis=0))
+    rate_col = as_column(jnp.broadcast_to(rates_ref[...], (size, HEADS)))
+    write_gate = jax.nn.sigmoid(write_col) * live
+    softplus = jnp.maximum(forget_col, 0.0) + jnp.log1p(jnp.exp(-jnp.abs(forget_col)))
+    forget = -jnp.exp(rate_col) * softplus * live
+    forget_row = to_row(forget)
+    cumulative = jnp.sum(jnp.where(causal, forget_row, 0.0), axis=1, keepdims=True)
+    final = jnp.sum(jnp.where(same, forget_row, 0.0), axis=1, keepdims=True)
+    decay = jnp.where(causal, jnp.exp(jnp.minimum(cumulative - to_row(cumulative), 0.0)), 0.0)
+    growth = jnp.exp(cumulative)
+    fading = jnp.exp(final - cumulative)
+    shrink = jnp.exp(final)
+
+    for copy in part_copies:
+        copy.wait_recv()
+
+    def by_head(index):
+        pieces = []
+        for j in range(devices):
+            block = part_recv[j, :, index * cols : (index + 1) * cols].astype(F32)
+            for at in range(0, cols, HEAD):
+                pieces.append(block[:, at : at + HEAD])
+        return jnp.concatenate(pieces, axis=0)
+
+    def dot(a, b, dims=((1,), (0,))):
+        return lax.dot_general(a, b, (dims, ((), ())), precision=HIGH, preferred_element_type=F32)
+
+    query, key_in, value, gating = (by_head(index) for index in range(4))
+    query_unit = (
+        query
+        * lax.rsqrt(jnp.sum(query * query, axis=1, keepdims=True) + EPSILON)
+        * (1.0 / math.sqrt(HEAD))
+    )
+    key_unit = key_in * lax.rsqrt(jnp.sum(key_in * key_in, axis=1, keepdims=True) + EPSILON)
+    lower = dot(key_unit, key_unit, ((1,), (1,)))
+    lower = jnp.where(strict, write_gate * decay * lower, 0.0)
+    squared = dot(lower, lower)
+    fourth = dot(squared, squared)
+    inverse = dot(identity - lower, identity + squared)
+    inverse = dot(inverse, identity + fourth)
+    target = dot(inverse, write_gate * value)
+    key_mix = dot(inverse, (write_gate * growth) * key_unit)
+    query_grown = query_unit * growth
+    scores = dot(query_unit, key_unit, ((1,), (1,))) * decay
+    loads["state"].wait()
+    key_terms, query_terms = [], []
+    for head in range(HEADS):
+        at = slice(head * BLK, (head + 1) * BLK)
+        both = jnp.concatenate([key_mix[at], query_grown[at]], axis=0)
+        result = dot(both, state[head])
+        key_terms.append(result[:BLK])
+        query_terms.append(result[BLK:])
+    update = target - jnp.concatenate(key_terms, axis=0)
+    attend = jnp.concatenate(query_terms, axis=0) + dot(scores, update)
+    normed = attend * lax.rsqrt(jnp.mean(attend * attend, axis=1, keepdims=True) + EPSILON)
+    normed = normed * jax.nn.silu(gating) * live
+    heads_all[me] = jnp.concatenate(
+        [normed[head * BLK : (head + 1) * BLK] for head in range(HEADS)], axis=1
+    ).astype(BF16)
+    copies = gather_start(2, heads_all)
+    faded = key_unit * fading
+    for head in range(HEADS):
+        at = slice(head * BLK, (head + 1) * BLK)
+        outer = dot(faded[at], update[at], ((0,), (0,)))
+        state_out[head] = shrink[head * BLK : head * BLK + 1] * state[head] + outer
+    store = pltpu.make_async_copy(state_out, new_state_hbm.at[0], store_sem)
+    store.start()
+    gather_finish(2, heads_all, copies)
+
+    mixed = heads_all[...].astype(F32).reshape(rows, HEADS * HEAD).astype(BF16)
+    loads["out"].wait()
+    half = HEADS * HEAD // 2
+    first = jnp.dot(mixed[:, :half], out_w[:half], preferred_element_type=F32).astype(BF16)
+    second = jnp.dot(mixed[:, half:], out_w[half:], preferred_element_type=F32).astype(BF16)
+    residual = gathers[1, me].astype(F32)
+    after_mix = (residual + (first.astype(F32) + second.astype(F32))).astype(BF16)
+    gathers[2, me] = after_mix
+    copies = gather_start(3, gathers.at[2])
+    gather_finish(3, gathers.at[2], copies)
+
+    total = half_step(1, gathers.at[2], gains2_ref, ("gate2", "up2", "down2"), gate2, up2, down2)
+    mixed_out_ref[...] = (gathers[2, me].astype(F32) + 0.5 * total).astype(BF16)
+    for copy in part_copies:
+        copy.wait_send()
+    store.wait()
+
+
+def fused_call(mesh, *args):
+    (
+        tokens, lengths, state, gain_first, first_gate, first_up, first_down, gain_mix,
+        query_weight, key_weight, value_weight, gating_weight, write_weight, forget_weight,
+        forget_rate, out_weight, gain_second, second_gate, second_up, second_down,
+    ) = args
+    kv_size = mesh.shape["kv"]
+    devices = kv_size * mesh.shape["tp"]
+    rows, cols = tokens.shape
+    channels = gain_first.shape[0]
+    hidden_local = first_gate.shape[1]
+    take = -(-hidden_local // 256) * 128
+    phases = 2
+    in_vmem = pl.BlockSpec(memory_space=pltpu.VMEM)
+    in_smem = pl.BlockSpec(memory_space=pltpu.SMEM)
+    in_any = pl.BlockSpec(memory_space=pl.ANY)
+    dma = pltpu.SemaphoreType.DMA
+    return pl.pallas_call(
+        functools.partial(fused_kernel, kv_size, channels),
+        out_shape=(
+            jax.ShapeDtypeStruct(tokens.shape, tokens.dtype),
+            jax.ShapeDtypeStruct(state.shape, state.dtype),
+        ),
+        in_specs=[in_vmem, in_smem] + [in_vmem] * 4 + [in_any] * 14,
+        out_specs=(in_vmem, in_any),
+        scratch_shapes=[
+            pltpu.VMEM((channels, take), BF16),
+            pltpu.VMEM((channels, take), BF16),
+            pltpu.VMEM((take, channels), BF16),
+            pltpu.VMEM((channels, take), BF16),
+            pltpu.VMEM((channels, take), BF16),
+            pltpu.VMEM((take, channels), BF16),
+            pltpu.VMEM((4,) + query_weight.shape, BF16),
+            pltpu.VMEM(out_weight.shape, BF16),
+            pltpu.VMEM(write_weight.shape, BF16),
+            pltpu.VMEM(forget_weight.shape, BF16),
+            pltpu.VMEM(state.shape[1:], F32),
+            pltpu.VMEM(state.shape[1:], F32),
+            pltpu.VMEM((rows, channels), BF16),
+            pltpu.VMEM((rows, 128), F32),
+            pltpu.VMEM((rows, 128), F32),
+            pltpu.VMEM((3, devices, rows, cols), BF16),
+            pltpu.VMEM((devices, BLK, HEADS * HEAD), BF16),
+            pltpu.VMEM((phases, kv_size, rows, cols), F32),
+            pltpu.VMEM((phases, kv_size, rows, cols), F32),
+            pltpu.VMEM((phases, kv_size, rows, cols), BF16),
+            pltpu.VMEM((phases, kv_size, rows, cols), BF16),
+            pltpu.VMEM((devices, BLK, 4 * cols), BF16),
+            pltpu.VMEM((devices, BLK, 4 * cols), BF16),
+            dma((14,)),
+            dma((4, 2 * kv_size)),
+            dma((4, 2 * kv_size)),
+            dma((phases, kv_size)),
+            dma((phases, kv_size)),
+            dma((phases, kv_size)),
+            dma((phases, kv_size)),
+            dma((devices,)),
+            dma((devices,)),
+            dma,
+        ],
+        compiler_params=pltpu.CompilerParams(
+            collective_id=0, has_side_effects=True, vmem_limit_bytes=VMEM_LIMIT
+        ),
+    )(
+        tokens, lengths, gain_first.reshape(1, -1), gain_mix.reshape(1, -1),
+        gain_second.reshape(1, -1), forget_rate.reshape(1, -1), state,
+        first_gate, first_up, first_down, query_weight, key_weight, value_weight,
+        gating_weight, write_weight, forget_weight, out_weight, second_gate, second_up,
+        second_down,
+    )
+
+
+def fits_fused(mesh, args):
+    tokens, lengths, state, first_gate = args[0], args[1], args[2], args[4]
+    rows, cols = tokens.shape
+    devices = mesh.shape["kv"] * mesh.shape["tp"]
+    return (
+        mesh.shape["tp"] == 2
+        and lengths.shape[0] == 1
+        and rows == devices * BLK
+        and cols % 256 == 0
+        and first_gate.shape[1] % 128 == 0
+        and state.shape[1:] == (HEADS, HEAD, HEAD)
+    )
+
+
 def solution(mesh):
     in_specs = (
         P("dp", ("kv", "tp")),
@@ -186,6 +659,12 @@
         P("kv", None),
     )
     out_specs = (P("dp", ("kv", "tp")), P(("dp", "kv", "tp"), None, None, None))
+
+    def body(*args):
+        if fits_fused(mesh, args):
+            return fused_call(mesh, *args)
+        return per_device(*args)
+
     return jax.shard_map(
-        per_device, mesh=mesh, in_specs=in_specs, out_specs=out_specs, check_vma=False
-    )
+        body, mesh=mesh, in_specs=in_specs, out_specs=out_specs, check_vma=False
+    )

time: 176 us -> 65.7 us (0.37)
  blocking collectives: 73.2 us -> 0 us
  Pallas kernels: 0 us -> 56.6 us
  waiting for transfers between devices: 42.3 us -> 0 us
  matrix products: 35.8 us -> 0 us
  between operations: 15.2 us -> 1.29 us
  local copies, waits for them, and re-layouts: 3.13 us -> 7.38 us
  starting transfers between devices: 3.45 us -> 0 us
  other arithmetic: 1.76 us -> 0 us
    all_gather x4 -> x0, blocking collectives: 57.2 us -> none  [the longest x2 28.6 us: feed_forward(): lax.all_gather(paired, 'kv', axis=1, tiled=True)]
    pallas_call x0 -> x1, Pallas kernels: none -> 56.6 us  [fused_call(): pl.pallas_call(functools.partial(fused_kernel, kv_size, channels), out_sh...]
    reduce_scatter x2 -> x0, waiting for transfers between devices: 36.9 us -> none  [feed_forward(): lax.psum_scatter(ffn_term, 'kv', scatter_dimension=1, tiled=True)]
    dot_general x24 -> x0, matrix products: 35.8 us -> none  [the longest x2 14.2 us: finish_units(): return jnp.dot(hidden, down_rows, preferred_element_type=jnp.float32)]
    all_to_all x4 -> x0, blocking collectives: 16.1 us -> none  [the longest x2 8.52 us: feed_forward(): lax.all_to_all(hidden_in, 'tp', split_axis=0, concat_axis=1, tiled=True)]
    unnamed x18 -> x4, local copies, waits for them, and re-layouts: 0.06 us -> 7.38 us
    all_to_all x1 -> x0, waiting for transfers between devices: 5.31 us -> none  [per_device(): lax.all_to_all(stacked.astype(jnp.bfloat16), ('kv', 'tp'), split_axis=1,...]
    all_to_all x1 -> x0, starting transfers between devices: 3.37 us -> none  [per_device(): lax.all_to_all(stacked.astype(jnp.bfloat16), ('kv', 'tp'), split_axis=1,...]
  transfers between devices with their start and end apart: 3 -> 0, of which waited for: 3 -> 0; matrix products, arithmetic and copies ran while one was open for 2% -> 0% of each run, Pallas kernels for 0% -> 0%
where the time goes in v1:
time: 65.7 us; the launch traced here: 65.3 us
  Pallas kernels  56.6 us (86%)
  local copies, waits for them, and re-layouts  7.38 us (11%)
  between operations  1.29 us (2%)
    pallas_call x1, Pallas kernels, fused_call(): pl.pallas_call(functools.partial(fused_kernel, kv_size, channels), out_sh...  56.6 us
    unnamed x4, local copies, waits for them, and re-layouts  7.38 us

profile of v1, /device:TPU:0, one launch (start us, length us, event | category | flops | bytes accessed | tf_op | source)
XLA Modules:
  0.0 65.3 jit_solution(7341100735125668110)
XLA Ops:
  1.3 1.8 %copy.22.write_hbm = bf16[2048,16]{1,0:T(8,128)(2,1)} copy(bf16[2048,16]{0,1:T(8,128)(2,1)} %param.32) | data formatting | bytes 131072 | tf_op args[12]
  3.1 1.9 %copy.23.forget_hbm = bf16[2048,16]{1,0:T(8,128)(2,1)} copy(bf16[2048,16]{0,1:T(8,128)(2,1)} %param.33) | data formatting | bytes 131072 | tf_op args[13]
  5.0 56.6 %shard_map.203 = (bf16[64,256]{1,0:T(8,128)(2,1)}, f32[1,16,128,128]{3,2,1,0:T(8,128)}) custom-call(bf16[64,256]{1,0:T(8,128)(2,1)} %tokens_ref.1, s32[1]{0:T(128)S(6)} %copy.26.lengths_ref, f32[1,2048]{1,0:T(1,128)} %bitcast.4, f32[1,2048]{1,0:T(1,128)} %bitcast.5, f32[1,2048]{1,0:T(1,128)} %bitcast.6, f32[1,16]{1,0:T(1,128)} %bitcast.7, ...), custom_call_target="tpu_custom_call" | custom-call | tf_op jit(solution)/shard_map/pallas_call | solution.py:569
  61.6 1.4 %copy.27 = bf16[64,256]{1,0:T(8,128)(2,1)} copy(bf16[64,256]{1,0:T(8,128)(2,1)} %get-tuple-element.4) | data formatting | bytes 65536
  63.0 2.3 %copy.28 = f32[1,16,128,128]{3,2,1,0:T(8,128)} copy(f32[1,16,128,128]{3,2,1,0:T(8,128)} %get-tuple-element.5) | data formatting | bytes 2097152

commit v2 on v1

--- a/solution.py
+++ b/solution.py
@@ -205,13 +205,15 @@
     down2,
     proj,
     out_w,
-    write_w,
-    forget_w,
+    small_w,
     state,
+    state_high,
+    state_low,
     state_out,
-    scaled,
-    wide,
-    narrow,
+    gate_acc,
+    up_acc,
+    proj_acc,
+    small_acc,
     gathers,
     heads_all,
     pair_send,
@@ -250,12 +252,12 @@
         "gate1": load(0, gate1_hbm.at[:, cut], gate1),
         "up1": load(1, up1_hbm.at[:, cut], up1),
         "down1": load(2, down1_hbm.at[cut, :], down1),
-        "query": load(3, query_hbm, proj.at[0]),
-        "key": load(4, key_hbm, proj.at[1]),
-        "value": load(5, value_hbm, proj.at[2]),
-        "gating": load(6, gating_hbm, proj.at[3]),
-        "write": load(7, write_hbm, write_w),
-        "forget": load(8, forget_hbm, forget_w),
+        "query": load(3, query_hbm, proj.at[:, 0:cols]),
+        "key": load(4, key_hbm, proj.at[:, cols : 2 * cols]),
+        "value": load(5, value_hbm, proj.at[:, 2 * cols : 3 * cols]),
+        "gating": load(6, gating_hbm, proj.at[:, 3 * cols : 4 * cols]),
+        "write": load(7, write_hbm, small_w.at[0:HEADS]),
+        "forget": load(8, forget_hbm, small_w.at[HEADS : 2 * HEADS]),
         "state": load(9, state_hbm.at[0], state),
         "out": load(10, out_hbm, out_w),
         "gate2": load(11, gate2_hbm.at[:, cut], gate2),
@@ -286,39 +288,37 @@
         )
     pl.semaphore_wait(barrier, devices - 1)
 
+    def swapped(off):
+        chip, bit = kv, 1
+        while bit < kv_size:
+            if off & bit:
+                chip = chip + bit - 2 * bit * lax.rem(kv // bit, 2)
+            bit *= 2
+        return chip
+
     def gather_start(phase, buf):
-        copies = []
-        for off in range(kv_size - 1, 0, -1):
-            copies.append(
-                remote(
-                    buf.at[me],
-                    buf.at[me],
-                    gather_send_sems.at[phase, off],
-                    gather_recv_sems.at[phase, off],
-                    lax.rem(kv + off, kv_size),
-                    tp,
-                )
-            )
-        copies.append(
-            remote(
+        copies = {}
+        for off in list(range(kv_size - 1, 0, -1)) + [0]:
+            copies[off] = remote(
                 buf.at[me],
                 buf.at[me],
-                gather_send_sems.at[phase, 0],
-                gather_recv_sems.at[phase, 0],
-                kv,
-                1 - tp,
+                gather_send_sems.at[phase, off],
+                gather_recv_sems.at[phase, off],
+                swapped(off),
+                1 - tp if off == 0 else tp,
             )
-        )
-        for copy in copies:
-            copy.start()
+            copies[off].start()
         return copies
 
-    def gather_finish(phase, buf, copies):
-        forwards = []
+    def gather_finish(phase, buf, copies, use=lambda slot, first: None):
+        use(me, True)
+        copies[0].wait_recv()
+        use(kv * 2 + 1 - tp, False)
+        forwards = {}
         for off in range(1, kv_size):
-            copies[kv_size - 1 - off].wait_recv()
-            slot = lax.rem(kv + kv_size - off, kv_size) * 2 + tp
-            forward = remote(
+            copies[off].wait_recv()
+            slot = swapped(off) * 2 + tp
+            forwards[off] = remote(
                 buf.at[slot],
                 buf.at[slot],
                 gather_send_sems.at[phase, kv_size - 1 + off],
@@ -326,29 +326,53 @@
                 kv,
                 1 - tp,
             )
-            forward.start()
-            forwards.append(forward)
-        copies[-1].wait_recv()
-        for forward in forwards:
-            forward.wait_recv()
-        for copy in copies + forwards:
-            copy.wait_send()
-
-    def scale_rows(buf, gain_ref):
-        squares = jnp.zeros((rows, 1), F32)
-        for j in range(devices):
-            values = buf[j].astype(F32)
-            squares = squares + jnp.sum(values * values, axis=1, keepdims=True)
-            gain = gain_ref[:, j * cols : (j + 1) * cols]
-            scaled[:, j * cols : (j + 1) * cols] = (values * gain).astype(BF16)
-        return lax.rsqrt(squares / channels + EPSILON)
-
-    def half_step(phase, buf, gain_ref, names, gate_w, up_w, down_w):
-        row_scale = scale_rows(buf, gain_ref)
+            forwards[off].start()
+        for off in range(1, kv_size):
+            use(swapped(off) * 2 + tp, False)
+        for off in range(1, kv_size):
+            forwards[off].wait_recv()
+            use(swapped(off) * 2 + 1 - tp, False)
+        for off in range(kv_size):
+            copies[off].wait_send()
+        for off in range(1, kv_size):
+            forwards[off].wait_send()
+
+    def multiply(buf, gain_ref, products):
+        squares = [jnp.zeros((rows, 1), F32)]
+
+        def use(slot, first):
+            at = pl.ds(pl.multiple_of(slot * cols, cols), cols)
+            values = buf[slot].astype(F32)
+            squares[0] = squares[0] + jnp.sum(values * values, axis=1, keepdims=True)
+            scaled = (values * gain_ref[:, at]).astype(BF16)
+            for acc, weight, across in products:
+                if across:
+                    term = lax.dot_general(
+                        scaled,
+                        weight[:, at],
+                        (((1,), (1,)), ((), ())),
+                        preferred_element_type=F32,
+                    )
+                else:
+                    term = jnp.dot(scaled, weight[at, :], preferred_element_type=F32)
+                if first:
+                    acc[...] = term
+                else:
+                    acc[...] += term
+
+        return squares, use
+
+    def inverse_rms(squares):
+        return lax.rsqrt(squares[0] / channels + EPSILON)
+
+    def half_step(phase, at, buf, copies, gain_ref, names, gate_w, up_w, down_w):
         loads[names[0]].wait()
-        gate = jnp.dot(scaled[...], gate_w[...], preferred_element_type=F32) * row_scale
         loads[names[1]].wait()
-        up = jnp.dot(scaled[...], up_w[...], preferred_element_type=F32) * row_scale
+        squares, use = multiply(buf, gain_ref, ((gate_acc, gate_w, False), (up_acc, up_w, False)))
+        gather_finish(at, buf, copies, use)
+        row_scale = inverse_rms(squares)
+        gate = gate_acc[...] * row_scale
+        up = up_acc[...] * row_scale
         column = lax.broadcasted_iota(jnp.int32, (rows, take), 1)
         hidden = jnp.where(column >= tp * overlap, jax.nn.silu(gate) * up, 0.0).astype(BF16)
         loads[names[2]].wait()
@@ -360,7 +384,7 @@
         order = list(range(kv_size - 1, -1, -1))
         pair_copies = []
         for off in order:
-            pair_send[phase, off] = columns_of(lax.rem(kv + off, kv_size), 1 - tp)
+            pair_send[phase, off] = columns_of(swapped(off), 1 - tp)
             copy = remote(
                 pair_send.at[phase, off],
                 pair_recv.at[phase, off],
@@ -374,7 +398,7 @@
         red_copies = []
         total = None
         for position, off in enumerate(order):
-            term = columns_of(lax.rem(kv + off, kv_size), tp)
+            term = columns_of(swapped(off), tp)
             pair_copies[position].wait_recv()
             term = term + pair_recv[phase, off]
             if off == 0:
@@ -386,7 +410,7 @@
                 red_recv.at[phase, off],
                 red_send_sems.at[phase, off],
                 red_recv_sems.at[phase, off],
-                lax.rem(kv + off, kv_size),
+                swapped(off),
                 tp,
             )
             copy.start()
@@ -403,22 +427,28 @@
     copies = gather_start(0, gathers.at[0])
     for name in ("query", "key", "value", "gating", "write", "forget", "state", "out"):
         loads[name].start()
-    gather_finish(0, gathers.at[0], copies)
     for name in ("gate2", "up2", "down2"):
         loads[name].start()
-    total = half_step(0, gathers.at[0], gains1_ref, ("gate1", "up1", "down1"), gate1, up1, down1)
+    total = half_step(
+        0, 0, gathers.at[0], copies, gains1_ref, ("gate1", "up1", "down1"), gate1, up1, down1
+    )
     after_first = (tokens_ref[...].astype(F32) + 0.5 * total).astype(BF16)
     gathers[1, me] = after_first
     copies = gather_start(1, gathers.at[1])
-    gather_finish(1, gathers.at[1], copies)
-
-    mix_scale = scale_rows(gathers.at[1], gains_mix_ref)
-    for index, name in enumerate(("query", "key", "value", "gating")):
+
+    loads["state"].wait()
+    for head in range(HEADS):
+        high = state[head].astype(BF16)
+        state_high[head] = high
+        state_low[head] = (state[head] - high.astype(F32)).astype(BF16)
+    for name in ("query", "key", "value", "gating", "write", "forget"):
         loads[name].wait()
-        product = jnp.dot(scaled[...], proj[index], preferred_element_type=F32) * mix_scale
-        part_send[:, :, index * cols : (index + 1) * cols] = product.reshape(
-            devices, BLK, cols
-        ).astype(BF16)
+    squares, use = multiply(
+        gathers.at[1], gains_mix_ref, ((proj_acc, proj, False), (small_acc, small_w, True))
+    )
+    gather_finish(1, gathers.at[1], copies, use)
+    mix_scale = inverse_rms(squares)
+    part_send[...] = (proj_acc[...] * mix_scale).reshape(devices, BLK, 4 * cols).astype(BF16)
     part_copies = []
     for off in range(1, devices):
         peer = lax.rem(me + off, devices)
@@ -433,13 +463,10 @@
         copy.start()
         part_copies.append(copy)
     part_recv[me] = part_send[me]
-    loads["write"].wait()
-    loads["forget"].wait()
-    wide[:, 0:HEADS] = jnp.dot(scaled[...], write_w[...], preferred_element_type=F32) * mix_scale
-    narrow[:, 0:HEADS] = jnp.dot(scaled[...], forget_w[...], preferred_element_type=F32) * mix_scale
+    small_acc[...] = small_acc[...] * mix_scale
     own = pl.ds(pl.multiple_of(me * BLK, BLK), BLK)
-    write_pre = wide[own, 0:HEADS]
-    forget_pre = narrow[own, 0:HEADS]
+    write_pre = small_acc[own, 0:HEADS]
+    forget_pre = small_acc[own, HEADS : 2 * HEADS]
 
     size = HEADS * BLK
     row = lax.broadcasted_iota(jnp.int32, (size, size), 0)
@@ -502,19 +529,27 @@
     fourth = dot(squared, squared)
     inverse = dot(identity - lower, identity + squared)
     inverse = dot(inverse, identity + fourth)
-    target = dot(inverse, write_gate * value)
-    key_mix = dot(inverse, (write_gate * growth) * key_unit)
+    key_grown = (write_gate * growth) * key_unit
     query_grown = query_unit * growth
     scores = dot(query_unit, key_unit, ((1,), (1,))) * decay
-    loads["state"].wait()
+
+    def cut_terms(a):
+        high = a.astype(BF16).astype(F32)
+        return high, a - high
+
     key_terms, query_terms = [], []
     for head in range(HEADS):
         at = slice(head * BLK, (head + 1) * BLK)
-        both = jnp.concatenate([key_mix[at], query_grown[at]], axis=0)
-        result = dot(both, state[head])
+        high, low = cut_terms(jnp.concatenate([key_grown[at], query_grown[at]], axis=0))
+        both = jnp.concatenate([high, low], axis=0).astype(BF16)
+        result = jnp.dot(both, state_high[head], preferred_element_type=F32)
+        result = result[: 2 * BLK] + result[2 * BLK :]
+        result = result + jnp.dot(
+            both[: 2 * BLK], state_low[head], preferred_element_type=F32
+        )
         key_terms.append(result[:BLK])
         query_terms.append(result[BLK:])
-    update = target - jnp.concatenate(key_terms, axis=0)
+    update = dot(inverse, write_gate * value - jnp.concatenate(key_terms, axis=0))
     attend = jnp.concatenate(query_terms, axis=0) + dot(scores, update)
     normed = attend * lax.rsqrt(jnp.mean(attend * attend, axis=1, keepdims=True) + EPSILON)
     normed = normed * jax.nn.silu(gating) * live
@@ -525,7 +560,14 @@
     faded = key_unit * fading
     for head in range(HEADS):
         at = slice(head * BLK, (head + 1) * BLK)
-        outer = dot(faded[at], update[at], ((0,), (0,)))
+        key_high, key_low = cut_terms(faded[at])
+        value_high, value_low = cut_terms(update[at])
+        outer = lax.dot_general(
+            jnp.concatenate([key_high, key_high, key_low], axis=0).astype(BF16),
+            jnp.concatenate([value_high, value_low, value_high], axis=0).astype(BF16),
+            (((0,), (0,)), ((), ())),
+            preferred_element_type=F32,
+        )
         state_out[head] = shrink[head * BLK : head * BLK + 1] * state[head] + outer
     store = pltpu.make_async_copy(state_out, new_state_hbm.at[0], store_sem)
     store.start()
@@ -540,9 +582,10 @@
     after_mix = (residual + (first.astype(F32) + second.astype(F32))).astype(BF16)
     gathers[2, me] = after_mix
     copies = gather_start(3, gathers.at[2])
-    gather_finish(3, gathers.at[2], copies)
-
-    total = half_step(1, gathers.at[2], gains2_ref, ("gate2", "up2", "down2"), gate2, up2, down2)
+
+    total = half_step(
+        1, 3, gathers.at[2], copies, gains2_ref, ("gate2", "up2", "down2"), gate2, up2, down2
+    )
     mixed_out_ref[...] = (gathers[2, me].astype(F32) + 0.5 * total).astype(BF16)
     for copy in part_copies:
         copy.wait_send()
@@ -566,7 +609,7 @@
     in_smem = pl.BlockSpec(memory_space=pltpu.SMEM)
     in_any = pl.BlockSpec(memory_space=pl.ANY)
     dma = pltpu.SemaphoreType.DMA
-    return pl.pallas_call(
+    mixed_out, new_state = pl.pallas_call(
         functools.partial(fused_kernel, kv_size, channels),
         out_shape=(
             jax.ShapeDtypeStruct(tokens.shape, tokens.dtype),
@@ -581,15 +624,17 @@
             pltpu.VMEM((channels, take), BF16),
             pltpu.VMEM((channels, take), BF16),
             pltpu.VMEM((take, channels), BF16),
-            pltpu.VMEM((4,) + query_weight.shape, BF16),
+            pltpu.VMEM((channels, 4 * cols), BF16),
             pltpu.VMEM(out_weight.shape, BF16),
-            pltpu.VMEM(write_weight.shape, BF16),
-            pltpu.VMEM(forget_weight.shape, BF16),
+            pltpu.VMEM((2 * HEADS, channels), BF16),
             pltpu.VMEM(state.shape[1:], F32),
+            pltpu.VMEM(state.shape[1:], BF16),
+            pltpu.VMEM(state.shape[1:], BF16),
             pltpu.VMEM(state.shape[1:], F32),
-            pltpu.VMEM((rows, channels), BF16),
-            pltpu.VMEM((rows, 128), F32),
-            pltpu.VMEM((rows, 128), F32),
+            pltpu.VMEM((rows, take), F32),
+            pltpu.VMEM((rows, take), F32),
+            pltpu.VMEM((rows, 4 * cols), F32),
+            pltpu.VMEM((rows, 2 * HEADS), F32),
             pltpu.VMEM((3, devices, rows, cols), BF16),
             pltpu.VMEM((devices, BLK, HEADS * HEAD), BF16),
             pltpu.VMEM((phases, kv_size, rows, cols), F32),
@@ -616,9 +661,48 @@
         tokens, lengths, gain_first.reshape(1, -1), gain_mix.reshape(1, -1),
         gain_second.reshape(1, -1), forget_rate.reshape(1, -1), state,
         first_gate, first_up, first_down, query_weight, key_weight, value_weight,
-        gating_weight, write_weight, forget_weight, out_weight, second_gate, second_up,
+        gating_weight, write_weight.T, forget_weight.T, out_weight, second_gate, second_up,
         second_down,
     )
+    return hand_out(mixed_out, new_state)
+
+
+def hand_out_kernel(mixed_ref, state_hbm, mixed_out_ref, state_out_hbm, held, in_sems, out_sems):
+    heads = held.shape[0]
+    count = in_sems.shape[0]
+    step = heads // count
+    takes, puts = [], []
+    for i in range(count):
+        at = pl.ds(i * step, step)
+        takes.append(pltpu.make_async_copy(state_hbm.at[0, at], held.at[at], in_sems.at[i]))
+        puts.append(pltpu.make_async_copy(held.at[at], state_out_hbm.at[0, at], out_sems.at[i]))
+        takes[i].start()
+    mixed_out_ref[...] = mixed_ref[...]
+    for i in range(count):
+        takes[i].wait()
+        puts[i].start()
+    for put in puts:
+        put.wait()
+
+
+def hand_out(mixed_out, new_state):
+    in_vmem = pl.BlockSpec(memory_space=pltpu.VMEM)
+    in_any = pl.BlockSpec(memory_space=pl.ANY)
+    return pl.pallas_call(
+        hand_out_kernel,
+        out_shape=(
+            jax.ShapeDtypeStruct(mixed_out.shape, mixed_out.dtype),
+            jax.ShapeDtypeStruct(new_state.shape, new_state.dtype),
+        ),
+        in_specs=[in_vmem, in_any],
+        out_specs=(in_vmem, in_any),
+        scratch_shapes=[
+            pltpu.VMEM(new_state.shape[1:], new_state.dtype),
+            pltpu.SemaphoreType.DMA((4,)),
+            pltpu.SemaphoreType.DMA((4,)),
+        ],
+        compiler_params=pltpu.CompilerParams(vmem_limit_bytes=VMEM_LIMIT),
+    )(mixed_out, new_state)
 
 
 def fits_fused(mesh, args):
@@ -627,6 +711,7 @@
     devices = mesh.shape["kv"] * mesh.shape["tp"]
     return (
         mesh.shape["tp"] == 2
+        and mesh.shape["kv"] & (mesh.shape["kv"] - 1) == 0
         and lengths.shape[0] == 1
         and rows == devices * BLK
         and cols % 256 == 0

time: 65.7 us -> 55.9 us (0.85)
  local copies, waits for them, and re-layouts: 7.38 us -> 0 us
  Pallas kernels: 56.6 us -> 54.3 us
    unnamed x4 -> x0, local copies, waits for them, and re-layouts: 7.38 us -> none
    pallas_call x1, Pallas kernels: 56.6 us -> 51 us  [fused_call(): pl.pallas_call(functools.partial(fused_kernel, kv_size, channels), out_sh...]
    pallas_call x0 -> x1, Pallas kernels: none -> 3.35 us  [hand_out(): pl.pallas_call(hand_out_kernel, out_shape=(jax.ShapeDtypeStruct(mixed_out...]
where the time goes in v2:
time: 55.9 us; the launch traced here: 55.6 us
  Pallas kernels  54.3 us (97%)
  between operations  1.29 us (2%)
    pallas_call x1, Pallas kernels, fused_call(): pl.pallas_call(functools.partial(fused_kernel, kv_size, channels), out_sh...  51 us
    pallas_call x1, Pallas kernels, hand_out(): pl.pallas_call(hand_out_kernel, out_shape=(jax.ShapeDtypeStruct(mixed_out...  3.35 us

profile of v2, /device:TPU:0, one launch (start us, length us, event | category | flops | bytes accessed | tf_op | source)
XLA Modules:
  0.0 55.6 jit_solution(16706025989256634979)
XLA Ops:
  1.3 51.0 %shard_map.203 = (bf16[64,256]{1,0:T(8,128)(2,1)}, f32[1,16,128,128]{3,2,1,0:T(8,128)}) custom-call(bf16[64,256]{1,0:T(8,128)(2,1)} %tokens_ref.1, s32[1]{0:T(128)S(6)} %copy.22.lengths_ref, f32[1,2048]{1,0:T(1,128)} %bitcast.8, f32[1,2048]{1,0:T(1,128)} %bitcast.9, f32[1,2048]{1,0:T(1,128)} %bitcast.10, f32[1,16]{1,0:T(1,128)} %bitcast.11, ...), custom_call_target="tpu_custom_call" | custom-call | tf_op jit(solution)/shard_map/pallas_call | solution.py:612
  52.3 3.4 %shard_map.204 = (bf16[64,256]{1,0:T(8,128)(2,1)}, f32[1,16,128,128]{3,2,1,0:T(8,128)}) custom-call(bf16[64,256]{1,0:T(8,128)(2,1)} %get-tuple-element.4.mixed_ref, f32[1,16,128,128]{3,2,1,0:T(8,128)} %get-tuple-element.5.state_hbm), custom_call_target="tpu_custom_call" | custom-call | tf_op jit(solution)/shard_map/pallas_call | solution.py:691

commit v3 on v2

--- a/solution.py
+++ b/solution.py
@@ -167,7 +167,6 @@
 
 F32 = jnp.float32
 BF16 = jnp.bfloat16
-HIGH = lax.Precision.HIGHEST
 MESH = pl.DeviceIdType.MESH
 VMEM_LIMIT = 60 * 1024 * 1024
 
@@ -175,12 +174,12 @@
 def fused_kernel(
     kv_size,
     channels,
-    tokens_ref,
+    tokens_hbm,
     lengths_ref,
-    gains1_ref,
-    gains_mix_ref,
-    gains2_ref,
-    rates_ref,
+    gains1_hbm,
+    gains_mix_hbm,
+    gains2_hbm,
+    rates_hbm,
     state_hbm,
     gate1_hbm,
     up1_hbm,
@@ -209,6 +208,10 @@
     state,
     state_high,
     state_low,
+    gains1_ref,
+    gains_mix_ref,
+    gains2_ref,
+    rates_ref,
     state_out,
     gate_acc,
     up_acc,
@@ -237,7 +240,7 @@
     tp = lax.axis_index("tp")
     devices = 2 * kv_size
     me = kv * 2 + tp
-    rows, cols = tokens_ref.shape
+    rows, cols = tokens_hbm.shape
     take = gate1.shape[1]
     hidden_local = gate1_hbm.shape[1]
     lead = hidden_local - take
@@ -263,8 +266,14 @@
         "gate2": load(11, gate2_hbm.at[:, cut], gate2),
         "up2": load(12, up2_hbm.at[:, cut], up2),
         "down2": load(13, down2_hbm.at[cut, :], down2),
+        "tokens": load(14, tokens_hbm, gathers.at[0, me]),
+        "gains1": load(15, gains1_hbm, gains1_ref),
+        "gains_mix": load(16, gains_mix_hbm, gains_mix_ref),
+        "gains2": load(17, gains2_hbm, gains2_ref),
+        "rates": load(18, rates_hbm, rates_ref),
     }
-    for name in ("gate1", "up1", "down1"):
+    small = ("tokens", "gains1", "gains_mix", "gains2", "rates")
+    for name in small + ("gate1", "up1", "down1"):
         loads[name].start()
 
     def remote(src, dst, send_sem, recv_sem, to_kv, to_tp):
@@ -288,6 +297,8 @@
         )
     pl.semaphore_wait(barrier, devices - 1)
 
+    sent = []
+
     def swapped(off):
         chip, bit = kv, 1
         while bit < kv_size:
@@ -305,7 +316,7 @@
                 gather_send_sems.at[phase, off],
                 gather_recv_sems.at[phase, off],
                 swapped(off),
-                1 - tp if off == 0 else tp,
+                1 - tp,
             )
             copies[off].start()
         return copies
@@ -317,7 +328,7 @@
         forwards = {}
         for off in range(1, kv_size):
             copies[off].wait_recv()
-            slot = swapped(off) * 2 + tp
+            slot = swapped(off) * 2 + 1 - tp
             forwards[off] = remote(
                 buf.at[slot],
                 buf.at[slot],
@@ -328,14 +339,12 @@
             )
             forwards[off].start()
         for off in range(1, kv_size):
-            use(swapped(off) * 2 + tp, False)
+            use(swapped(off) * 2 + 1 - tp, False)
         for off in range(1, kv_size):
             forwards[off].wait_recv()
-            use(swapped(off) * 2 + 1 - tp, False)
-        for off in range(kv_size):
-            copies[off].wait_send()
-        for off in range(1, kv_size):
-            forwards[off].wait_send()
+            use(swapped(off) * 2 + tp, False)
+        sent.extend(copies.values())
+        sent.extend(forwards.values())
 
     def multiply(buf, gain_ref, products):
         squares = [jnp.zeros((rows, 1), F32)]
@@ -384,7 +393,7 @@
         order = list(range(kv_size - 1, -1, -1))
         pair_copies = []
         for off in order:
-            pair_send[phase, off] = columns_of(swapped(off), 1 - tp)
+            pair_send[phase, off] = columns_of(swapped(off), tp if off else 1 - tp)
             copy = remote(
                 pair_send.at[phase, off],
                 pair_recv.at[phase, off],
@@ -398,7 +407,7 @@
         red_copies = []
         total = None
         for position, off in enumerate(order):
-            term = columns_of(swapped(off), tp)
+            term = columns_of(swapped(off), 1 - tp if off else tp)
             pair_copies[position].wait_recv()
             term = term + pair_recv[phase, off]
             if off == 0:
@@ -411,7 +420,7 @@
                 red_send_sems.at[phase, off],
                 red_recv_sems.at[phase, off],
                 swapped(off),
-                tp,
+                1 - tp,
             )
             copy.start()
             red_copies.append(copy)
@@ -419,11 +428,11 @@
             copy.wait_recv()
         for off in range(1, kv_size):
             total = total + red_recv[phase, off].astype(F32)
-        for copy in pair_copies + red_copies:
-            copy.wait_send()
+        sent.extend(pair_copies + red_copies)
         return total
 
-    gathers[0, me] = tokens_ref[...]
+    for name in small:
+        loads[name].wait()
     copies = gather_start(0, gathers.at[0])
     for name in ("query", "key", "value", "gating", "write", "forget", "state", "out"):
         loads[name].start()
@@ -432,7 +441,7 @@
     total = half_step(
         0, 0, gathers.at[0], copies, gains1_ref, ("gate1", "up1", "down1"), gate1, up1, down1
     )
-    after_first = (tokens_ref[...].astype(F32) + 0.5 * total).astype(BF16)
+    after_first = (gathers[0, me].astype(F32) + 0.5 * total).astype(BF16)
     gathers[1, me] = after_first
     copies = gather_start(1, gathers.at[1])
 
@@ -513,8 +522,19 @@
                 pieces.append(block[:, at : at + HEAD])
         return jnp.concatenate(pieces, axis=0)
 
-    def dot(a, b, dims=((1,), (0,))):
-        return lax.dot_general(a, b, (dims, ((), ())), precision=HIGH, preferred_element_type=F32)
+    def cut_terms(a):
+        high = a.astype(BF16).astype(F32)
+        return high, a - high
+
+    def dot(a, b, across=False):
+        high_a, low_a = cut_terms(a)
+        high_b, low_b = cut_terms(b)
+        axis = 1 if across else 0
+        left = jnp.concatenate([high_a, high_a, low_a], axis=1).astype(BF16)
+        right = jnp.concatenate([high_b, low_b, high_b], axis=axis).astype(BF16)
+        return lax.dot_general(
+            left, right, (((1,), (axis,)), ((), ())), preferred_element_type=F32
+        )
 
     query, key_in, value, gating = (by_head(index) for index in range(4))
     query_unit = (
@@ -523,7 +543,8 @@
         * (1.0 / math.sqrt(HEAD))
     )
     key_unit = key_in * lax.rsqrt(jnp.sum(key_in * key_in, axis=1, keepdims=True) + EPSILON)
-    lower = dot(key_unit, key_unit, ((1,), (1,)))
+    products = dot(jnp.concatenate([key_unit, query_unit], axis=0), key_unit, True)
+    lower = products[:size]
     lower = jnp.where(strict, write_gate * decay * lower, 0.0)
     squared = dot(lower, lower)
     fourth = dot(squared, squared)
@@ -531,11 +552,7 @@
     inverse = dot(inverse, identity + fourth)
     key_grown = (write_gate * growth) * key_unit
     query_grown = query_unit * growth
-    scores = dot(query_unit, key_unit, ((1,), (1,))) * decay
-
-    def cut_terms(a):
-        high = a.astype(BF16).astype(F32)
-        return high, a - high
+    scores = products[size:] * decay
 
     key_terms, query_terms = [], []
     for head in range(HEADS):
@@ -587,7 +604,7 @@
         1, 3, gathers.at[2], copies, gains2_ref, ("gate2", "up2", "down2"), gate2, up2, down2
     )
     mixed_out_ref[...] = (gathers[2, me].astype(F32) + 0.5 * total).astype(BF16)
-    for copy in part_copies:
+    for copy in part_copies + sent:
         copy.wait_send()
     store.wait()
 
@@ -615,7 +632,7 @@
             jax.ShapeDtypeStruct(tokens.shape, tokens.dtype),
             jax.ShapeDtypeStruct(state.shape, state.dtype),
         ),
-        in_specs=[in_vmem, in_smem] + [in_vmem] * 4 + [in_any] * 14,
+        in_specs=[in_any, in_smem] + [in_any] * 18,
         out_specs=(in_vmem, in_any),
         scratch_shapes=[
             pltpu.VMEM((channels, take), BF16),
@@ -630,6 +647,10 @@
             pltpu.VMEM(state.shape[1:], F32),
             pltpu.VMEM(state.shape[1:], BF16),
             pltpu.VMEM(state.shape[1:], BF16),
+            pltpu.VMEM((1, channels), F32),
+            pltpu.VMEM((1, channels), F32),
+            pltpu.VMEM((1, channels), F32),
+            pltpu.VMEM((1, HEADS), F32),
             pltpu.VMEM(state.shape[1:], F32),
             pltpu.VMEM((rows, take), F32),
             pltpu.VMEM((rows, take), F32),
@@ -643,7 +664,7 @@
             pltpu.VMEM((phases, kv_size, rows, cols), BF16),
             pltpu.VMEM((devices, BLK, 4 * cols), BF16),
             pltpu.VMEM((devices, BLK, 4 * cols), BF16),
-            dma((14,)),
+            dma((19,)),
             dma((4, 2 * kv_size)),
             dma((4, 2 * kv_size)),
             dma((phases, kv_size)),
@@ -667,26 +688,26 @@
     return hand_out(mixed_out, new_state)
 
 
-def hand_out_kernel(mixed_ref, state_hbm, mixed_out_ref, state_out_hbm, held, in_sems, out_sems):
+def hand_out_kernel(mixed_hbm, state_hbm, mixed_out_hbm, state_out_hbm, mixed, held, in_sems, out_sems):
     heads = held.shape[0]
-    count = in_sems.shape[0]
+    count = in_sems.shape[0] - 1
     step = heads // count
-    takes, puts = [], []
+    takes = [pltpu.make_async_copy(mixed_hbm, mixed, in_sems.at[count])]
+    puts = [pltpu.make_async_copy(mixed, mixed_out_hbm, out_sems.at[count])]
     for i in range(count):
         at = pl.ds(i * step, step)
         takes.append(pltpu.make_async_copy(state_hbm.at[0, at], held.at[at], in_sems.at[i]))
         puts.append(pltpu.make_async_copy(held.at[at], state_out_hbm.at[0, at], out_sems.at[i]))
-        takes[i].start()
-    mixed_out_ref[...] = mixed_ref[...]
-    for i in range(count):
-        takes[i].wait()
-        puts[i].start()
+    for take in takes:
+        take.start()
+    for take, put in zip(takes, puts):
+        take.wait()
+        put.start()
     for put in puts:
         put.wait()
 
 
 def hand_out(mixed_out, new_state):
-    in_vmem = pl.BlockSpec(memory_space=pltpu.VMEM)
     in_any = pl.BlockSpec(memory_space=pl.ANY)
     return pl.pallas_call(
         hand_out_kernel,
@@ -694,12 +715,13 @@
             jax.ShapeDtypeStruct(mixed_out.shape, mixed_out.dtype),
             jax.ShapeDtypeStruct(new_state.shape, new_state.dtype),
         ),
-        in_specs=[in_vmem, in_any],
-        out_specs=(in_vmem, in_any),
+        in_specs=[in_any, in_any],
+        out_specs=(in_any, in_any),
         scratch_shapes=[
+            pltpu.VMEM(mixed_out.shape, mixed_out.dtype),
             pltpu.VMEM(new_state.shape[1:], new_state.dtype),
-            pltpu.SemaphoreType.DMA((4,)),
-            pltpu.SemaphoreType.DMA((4,)),
+            pltpu.SemaphoreType.DMA((5,)),
+            pltpu.SemaphoreType.DMA((5,)),
         ],
         compiler_params=pltpu.CompilerParams(vmem_limit_bytes=VMEM_LIMIT),
     )(mixed_out, new_state)

time: 55.9 us -> 51.6 us (0.923)
  Pallas kernels: 54.3 us -> 50.1 us
    pallas_call x1, Pallas kernels: 51 us -> 48.1 us  [fused_call(): pl.pallas_call(functools.partial(fused_kernel, kv_size, channels), out_sh...]
    pallas_call x1, Pallas kernels: 3.35 us -> 2.02 us  [hand_out(): pl.pallas_call(hand_out_kernel, out_shape=(jax.ShapeDtypeStruct(mixed_out...]
where the time goes in v3:
time: 51.6 us; the launch traced here: 51.4 us
  Pallas kernels  50.1 us (97%)
  between operations  1.29 us (2%)
    pallas_call x1, Pallas kernels, fused_call(): pl.pallas_call(functools.partial(fused_kernel, kv_size, channels), out_sh...  48.1 us
    pallas_call x1, Pallas kernels, hand_out(): pl.pallas_call(hand_out_kernel, out_shape=(jax.ShapeDtypeStruct(mixed_out...  2.02 us

profile of v3, /device:TPU:0, one launch (start us, length us, event | category | flops | bytes accessed | tf_op | source)
XLA Modules:
  0.0 51.4 jit_solution(8648459061355471020)
XLA Ops:
  1.3 48.1 %shard_map.203 = (bf16[64,256]{1,0:T(8,128)(2,1)}, f32[1,16,128,128]{3,2,1,0:T(8,128)}) custom-call(bf16[64,256]{1,0:T(8,128)(2,1)} %tokens_hbm.1, s32[1]{0:T(128)S(6)} %copy.22.lengths_ref, f32[1,2048]{1,0:T(1,128)} %bitcast.8, f32[1,2048]{1,0:T(1,128)} %bitcast.9, f32[1,2048]{1,0:T(1,128)} %bitcast.10, f32[1,16]{1,0:T(1,128)} %bitcast.11, ...), custom_call_target="tpu_custom_call" | custom-call | tf_op jit(solution)/shard_map/pallas_call | solution.py:629
  49.4 2.0 %shard_map.204 = (bf16[64,256]{1,0:T(8,128)(2,1)}, f32[1,16,128,128]{3,2,1,0:T(8,128)}) custom-call(bf16[64,256]{1,0:T(8,128)(2,1)} %get-tuple-element.4.mixed_hbm, f32[1,16,128,128]{3,2,1,0:T(8,128)} %get-tuple-element.5.state_hbm), custom_call_target="tpu_custom_call" | custom-call | tf_op jit(solution)/shard_map/pallas_call | solution.py:712
